TPU v7x, 32 devices: a whole 2x2x4 slice. The times are simulated.
32 devices in a mesh: sp: 8 (over z, y), tp: 4 (over x, core).
Axes of the slice: x: 2, y: 2, z: 4, core: 2. Of those that a mesh axis runs over, the one named last changes fastest.
Arguments:
- tokens: bfloat16 [3072, 2048], P('sp', 'tp'), may hold values from -6 to 6
- norm_gain: float32 [2048], replicated, may hold values from 0.1 to 1.9
- w_glu_value: bfloat16 [2048, 2048], P(None, 'tp'), may hold values from -0.125 to 0.125
- w_glu_gate: bfloat16 [2048, 2048], P(None, 'tp'), may hold values from -0.125 to 0.125
- w_query: bfloat16 [2048, 2048], P(None, 'tp'), may hold values from -0.125 to 0.125
- w_key: bfloat16 [2048, 2048], P(None, 'tp'), may hold values from -0.125 to 0.125
- w_value: bfloat16 [2048, 2048], P(None, 'tp'), may hold values from -0.125 to 0.125
- score_offset: float32 [32], P('tp'), may hold values from -15 to -4, as said below
- conv_taps: bfloat16 [31, 2048], P(None, 'tp'), may hold values from -1 to 1
- conv_gain: float32 [2048], replicated, may hold values from 0.1 to 1.9
- w_conv_out: bfloat16 [2048, 2048], P(None, 'tp'), may hold values from -0.125 to 0.125
- w_attn_out: bfloat16 [2048, 2048], P(None, 'tp'), may hold values from -1 to 1
- w_gate_conv: bfloat16 [2048, 2048], P(None, 'tp'), may hold values from -0.125 to 0.125
- w_gate_attn: bfloat16 [2048, 2048], P(None, 'tp'), may hold values from -0.125 to 0.125
Outputs:
- mixed: bfloat16 [3072, 2048], P('sp', 'tp')
- log_weight: float32 [32, 3072], P('tp', 'sp')
Inputs may be any that keep to these rules, and one draw needn't show every extreme that they name: `score_offset`: per-head score offsets.
All inputs are finite; a program needn't handle non-finite values.
Results may differ from a plain program's by a relative error of at most 0.0078.
Values may be sent and summed in bfloat16 or wider, within the bound.
A program may use at most 128 MiB of HBM per device.

v0:
```python
import jax
import jax.numpy as jnp
from jax import lax
from jax.sharding import PartitionSpec as P

HEAD = 64
WIDTH = 31
key_span = 512


def passed_along(array, axis, by):
    length = lax.axis_size(axis)
    pairs = [(i, i + by) for i in range(length) if 0 <= i + by < length]
    return lax.ppermute(array, axis, pairs)


def sweep_block(
    sweep_state, key_block, value_block, key_first, query_first, query_heads, offsets, score_scale
):
    summed, spent_stick = sweep_state
    head_count = offsets.shape[0]
    query_count = query_heads.shape[0]
    key_count = key_block.shape[0]
    key_heads = key_block.reshape(key_count, head_count, -1)
    value_heads = value_block.reshape(key_count, head_count, -1)
    scores = (
        jnp.einsum("thd,shd->hts", query_heads, key_heads, preferred_element_type=jnp.float32)
        * score_scale
        + offsets[:, None, None]
    )
    query_pos = query_first + lax.iota(jnp.int32, query_count)
    key_pos = key_first + lax.iota(jnp.int32, key_count)
    allowed = (key_pos[None, :] <= query_pos[:, None]) & (key_pos[None, :] >= 0)
    softened = jnp.where(allowed[None], jax.nn.softplus(scores), 0.0)
    behind = lax.cumsum(softened, axis=2, reverse=True)
    stick = jnp.where(
        allowed[None], jnp.exp(scores - behind - spent_stick[:, :, None]), 0.0
    ).astype(jnp.bfloat16)
    summed = summed + jnp.einsum(
        "hts,shd->thd", stick, value_heads, preferred_element_type=jnp.float32
    )
    return (summed, spent_stick + behind[:, :, 0])


def body(
    tokens,
    norm_gain,
    w_glu_value,
    w_glu_gate,
    w_query,
    w_key,
    w_value,
    score_offset,
    conv_taps,
    conv_gain,
    w_conv_out,
    w_attn_out,
    w_gate_conv,
    w_gate_attn,
):
    whole_rows = lax.all_gather(tokens, "tp", axis=1, tiled=True)
    features = whole_rows.astype(jnp.float32)
    normed = (
        features
        * lax.rsqrt(jnp.mean(features * features, axis=-1, keepdims=True) + 1e-06)
        * norm_gain
    ).astype(jnp.bfloat16)
    glued = (
        jnp.dot(normed, w_glu_value, preferred_element_type=jnp.float32)
        * jax.nn.sigmoid(jnp.dot(normed, w_glu_gate, preferred_element_type=jnp.float32))
    ).astype(jnp.bfloat16)
    queries = jnp.dot(normed, w_query, preferred_element_type=jnp.float32).astype(jnp.bfloat16)
    keys = jnp.dot(normed, w_key, preferred_element_type=jnp.float32).astype(jnp.bfloat16)
    values = jnp.dot(normed, w_value, preferred_element_type=jnp.float32).astype(jnp.bfloat16)
    tok_rows = whole_rows.shape[0]
    tap_count = conv_taps.shape[0]
    channels = glued.shape[1]
    previous = passed_along(glued[tok_rows - (tap_count - 1) :], "sp", 1)
    extended = jnp.concatenate([previous, glued], axis=0)
    tap_rows = conv_taps.astype(jnp.float32)
    convolved = jnp.zeros((tok_rows, channels), jnp.float32)
    for tap in range(WIDTH):
        convolved = convolved + tap_rows[tap] * extended[tap : tap + tok_rows].astype(jnp.float32)
    convolved = convolved.astype(jnp.bfloat16)
    head_count = score_offset.shape[0]
    head_width = queries.shape[1] // head_count
    score_scale = 1.0 / HEAD**0.5
    query_heads = queries.reshape(tok_rows, head_count, head_width)
    own_index = lax.axis_index("sp")
    query_first = own_index * tok_rows
    start_state = (
        jnp.zeros((tok_rows, head_count, head_width), jnp.float32),
        jnp.zeros((head_count, tok_rows), jnp.float32),
    )
    gathered = (
        lax.all_gather(keys, "sp", axis=0, tiled=True),
        lax.all_gather(values, "sp", axis=0, tiled=True),
    )
    leading = jnp.zeros((key_span, keys.shape[1]), jnp.bfloat16)
    all_keys = jnp.concatenate([leading, gathered[0]], axis=0)
    all_values = jnp.concatenate([leading, gathered[1]], axis=0)
    key_end = (own_index + 1) * tok_rows
    turns = (key_end + key_span - 1) // key_span

    def advance(turn_index, sweep_state):
        key_first = key_end - (turn_index + 1) * key_span
        key_block = lax.dynamic_slice_in_dim(all_keys, key_first + key_span, key_span, 0)
        value_block = lax.dynamic_slice_in_dim(all_values, key_first + key_span, key_span, 0)
        return sweep_block(
            sweep_state,
            key_block,
            value_block,
            key_first,
            query_first,
            query_heads,
            score_offset,
            score_scale,
        )

    summed, spent_stick = lax.fori_loop(0, turns, advance, start_state)
    attended = summed.reshape(tok_rows, head_count * head_width).astype(jnp.bfloat16)
    log_weight = jnp.log(-jnp.expm1(-spent_stick))
    gate_conv = jax.nn.sigmoid(jnp.dot(normed, w_gate_conv, preferred_element_type=jnp.float32))
    gate_attn = jax.nn.sigmoid(jnp.dot(normed, w_gate_attn, preferred_element_type=jnp.float32))
    all_channels = conv_gain.shape[0]
    conv_float = convolved.astype(jnp.float32)
    channel_sum, channel_squares = lax.psum(
        (
            jnp.sum(conv_float, axis=-1, keepdims=True),
            jnp.sum(conv_float * conv_float, axis=-1, keepdims=True),
        ),
        "tp",
    )
    channel_mean = channel_sum / all_channels
    channel_var = channel_squares / all_channels - channel_mean * channel_mean
    local_gain = lax.dynamic_slice_in_dim(conv_gain, lax.axis_index("tp") * channels, channels, 0)
    conv_act = jax.nn.silu(
        (conv_float - channel_mean) * lax.rsqrt(channel_var + 1e-05) * local_gain
    ).astype(jnp.bfloat16)
    conv_piece = lax.all_gather(conv_act, "tp", axis=1, tiled=True)
    attn_piece = lax.all_gather(attended, "tp", axis=1, tiled=True)
    conv_branch = jnp.dot(conv_piece, w_conv_out, preferred_element_type=jnp.float32)
    attn_branch = jnp.dot(attn_piece, w_attn_out, preferred_element_type=jnp.float32)
    mixed = (gate_conv * conv_branch + gate_attn * attn_branch).astype(jnp.bfloat16)
    return (mixed, log_weight)


def solution(mesh):
    in_specs = (
        P("sp", "tp"),
        P(),
        P(None, "tp"),
        P(None, "tp"),
        P(None, "tp"),
        P(None, "tp"),
        P(None, "tp"),
        P("tp"),
        P(None, "tp"),
        P(),
        P(None, "tp"),
        P(None, "tp"),
        P(None, "tp"),
        P(None, "tp"),
    )
    out_specs = (P("sp", "tp"), P("tp", "sp"))
    return jax.shard_map(body, mesh=mesh, in_specs=in_specs, out_specs=out_specs, check_vma=False)
```

profile of v0, /device:TPU:0, one launch (start us, length us, event | category | flops | bytes accessed | tf_op | source)
XLA Modules:
  0.0 368.4 jit_solution(1898526458880367663)
XLA Ops:
  7.2 0.0 all-gather.6.cloned.1.call-start
  7.2 0.7 all-gather.6.cloned.1.call-update
  7.9 0.0 all-gather.10.cloned.1.call-start
  8.0 24.0 %all-gather.6.cloned.1.call-done = bf16[384,2048]{1,0:T(8,128)(2,1)} async-done(((bf16[384,512]{1,0:T(8,128)(2,1)}), bf16[384,2048]{1,0:T(8,128)(2,1)}) %all-gather.6.cloned.1.call-update) | async-done | bytes 1572880 | tf_op jit(solution)/shard_map/all_gather | solution.py:61
  31.9 1.8 fusion.22
  33.8 3.2 convolution_convert_fusion.2
  36.9 0.0 all-gather.10.cloned.1.call-update
  37.0 0.0 all-gather.12.cloned.1.call-start
  37.0 4.0 %convolution_convert_fusion.1 = bf16[384,512]{1,0:T(8,128)(2,1)} fusion(bf16[2048,512]{1,0:T(8,128)(2,1)} %param.21, bf16[384,2048]{1,0:T(8,128)(2,1)} %all-gather.6.cloned.1.call-done, f32[2048]{0:T(1024)S(1)} %copy-done.8, f32[384]{0:T(512)S(1)} %add_rsqrt_fusion), kind=kOutput, calls=%fused_computation.84 | convolution fusion | flops 808648704 | bytes 4072960 | tf_op jit(solution)/shard_map/dot_general | solution.py:73
  41.0 0.0 all-gather.12.cloned.1.call-update
  41.0 0.0 all-gather.14.cloned.1.call-start
  41.1 2.6 convolution_convert_fusion
  43.7 0.2 copy.25
  43.9 53.2 %all-gather.10.cloned.1.call-done = bf16[3072,512]{1,0:T(8,128)(2,1)} async-done(((bf16[384,512]{1,0:T(8,128)(2,1)}), bf16[3072,512]{1,0:T(8,128)(2,1)}) %all-gather.10.cloned.1.call-update) | async-done | bytes 3145744 | tf_op jit(solution)/shard_map/all_gather | solution.py:97
  97.1 3.9 %concatenate.10 = bf16[3584,512]{1,0:T(8,128)(2,1)} pad(bf16[3072,512]{1,0:T(8,128)(2,1)} %all-gather.10.cloned.1.call-done, bf16[]{:T(256)} %constant.89.clone.1), padding=512_0x0_0 | pad | bytes 6815746 | tf_op jit(solution)/shard_map/concatenate | solution.py:101
  101.1 57.0 %all-gather.12.cloned.1.call-done = bf16[3072,512]{1,0:T(8,128)(2,1)} async-done(((bf16[384,512]{1,0:T(8,128)(2,1)}), bf16[3072,512]{1,0:T(8,128)(2,1)}) %all-gather.12.cloned.1.call-update) | async-done | bytes 3145744 | tf_op jit(solution)/shard_map/all_gather | solution.py:96
  158.0 3.9 %concatenate.11 = bf16[3584,512]{1,0:T(8,128)(2,1)} pad(bf16[3072,512]{1,0:T(8,128)(2,1)} %all-gather.12.cloned.1.call-done, bf16[]{:T(256)} %constant.89.clone.1), padding=512_0x0_0 | pad | bytes 6815746 | tf_op jit(solution)/shard_map/concatenate | solution.py:100
  162.0 0.1 broadcast_in_dim.43
  162.1 25.8 %while.14 = (s32[]{:T(128)}, f32[384,8,64]{0,2,1:T(8,128)S(1)}, f32[8,384]{1,0:T(8,128)S(1)}, s32[]{:T(128)}, s32[]{:T(128)}, /*index=5*/bf16[3584,512]{1,0:T(8,...) while((s32[]{:T(128)}, f32[384,8,64]{0,2,1:T(8,128)S(1)}, ...), condition=%wide.region_8.9_spmd, body=%wide.region_5.8_spmd.sunk | while | flops 628213632 | bytes 71053592 | solution.py:120
  162.3 1.3 constant_dynamic-slice_fusion.3
  163.6 0.2 copy.42
  163.8 0.2 compare_and_fusion.2
  164.0 0.2 copy.43
  164.3 4.7 %fusion.112 = (f32[8,384,512]{1,2,0:T(8,128)S(1)}, f32[8,512,384]{2,1,0:T(8,128)S(1)}) fusion(f32[8]{0:T(128)S(1)} %get-tuple-element.322, pred[384,512]{0,1:T(8,128)(4,1)S(1)} %compare_and_fusion.2, bf16[512,8,64]{0,2,1:T(8,128)(2,1)S(1)} %bitcast.118, bf16[384,8,64]{0,2,1:T(8,128)(2,1)S(1)} %get-tuple-element.321), kind=kOutput, calls=%fused_computation.1.clone.1 | convolution fusion | flops 215482368 | bytes 13697056 | tf_op jit(solution)/shard_map/while/body/thd,shd->hts/dot_general | solution.py:27
  169.0 15.1 %fusion.113 = f32[8,384,4,128]{1,0,3,2:T(8,128)S(1)} fusion(f32[8,384,4,128]{1,3,2,0:T(8,128)S(1)} %bitcast.116), kind=kOutput, calls=%fused_computation.13.clone.1 | output fusion | flops 199753728 | bytes 12582912 | tf_op jit(solution)/shard_map/reduce-window.6
  184.1 0.1 fusion.114
  184.2 0.4 broadcast_add_fusion.2
  184.6 1.2 copy.44
  185.9 2.0 fusion.115
  187.9 0.8 convert_element_type.179
  188.7 0.0 all-gather.14.cloned.1.call-update
  188.7 0.3 all-gather.8.cloned.1.call-start
  189.1 3.3 fusion.31
  192.4 1.0 fusion.35
  193.5 28.1 %collective-permute-start = (bf16[30,512]{1,0:T(8,128)(2,1)S(1)}, bf16[30,512]{1,0:T(8,128)(2,1)S(1)}, u32[]{:S(2)}, u32[]{:S(2)}) collective-permute-start(bf16[30,512]{1,0:T(8,128)(2,1)S(1)} %slice.270), channel_id=1, source_target_pairs={{0,4},{4,8},{8,12},{12,16},{16,20},{20,24},{24,28},{1,5},{5,9},{9,... | collective-permute-start | bytes 92168 | tf_op jit(solution)/shard_map/ppermute | solution.py:14
  221.6 0.8 dynamic_slice.15
  222.4 0.8 collective-permute-done
  223.2 3.7 %convert_reduce_fusion = (f32[384]{0:T(512)S(1)}, f32[384]{0:T(512)S(1)}, bf16[384,512]{1,0:T(8,128)(2,1)S(1)}) fusion(bf16[384,512]{1,0:T(8,128)(2,1)S(1)} %fusion.35, f32[512]{0:T(512)S(1)} %bitcast.151, bf16[30,512]{1,0:T(8,128)(2,1)S(1)} %collective-permute-done, f32[512]{0:T(512)S(1)} %bitcast.150, f32[512]{0:T(512)S(1)} %bitcast.149, ...), kind=kLoop, calls=%fused_computation.88 | loop fusion | flops 36764928 | bytes 883712 | tf_op jit(solution)/shard_map/reduce_sum | solution.py:129
  226.9 5.7 %all-reduce.2 = (f32[384,1]{0,1:T(1,128)S(1)}, f32[384,1]{0,1:T(1,128)S(1)}) all-reduce(f32[384,1]{0,1:T(1,128)S(1)} %broadcast_in_dim.41, f32[384,1]{0,1:T(1,128)S(1)} %broadcast_in_dim.42), channel_id=1, replica_groups=mesh['sp'=8,'tp'=4] {'tp'}, use_global_device_ids=true, to_apply=%region_2.3 | all-reduce | flops 768 | bytes 6144 | tf_op jit(solution)/shard_map/psum | solution.py:127
  232.6 1.1 fusion.44
  233.7 0.0 all-gather.8.cloned.1.call-update
  233.8 2.9 fusion.33
  236.7 2.0 fusion.29
  238.7 0.6 negate_log_fusion
  239.3 96.0 %all-gather.14.cloned.1.call-done = bf16[384,2048]{0,1:T(8,128)(2,1)} async-done(((bf16[384,512]{0,1:T(8,128)(2,1)}), bf16[384,2048]{0,1:T(8,128)(2,1)}) %all-gather.14.cloned.1.call-update) | async-done | bytes 1572880 | tf_op jit(solution)/shard_map/all_gather | solution.py:141
  335.3 4.1 %convolution_multiply_fusion = f32[384,512]{1,0:T(8,128)} fusion(f32[384,512]{1,0:T(8,128)S(1)} %fusion.33, bf16[384,2048]{0,1:T(8,128)(2,1)} %all-gather.14.cloned.1.call-done, bf16[2048,512]{1,0:T(8,128)(2,1)} %param.27), kind=kOutput, calls=%fused_computation.71 | convolution fusion | flops 805502976 | bytes 5242880 | tf_op jit(solution)/shard_map/dot_general | solution.py:143
  339.4 18.2 %all-gather.8.cloned.1.call-done = bf16[384,2048]{1,0:T(8,128)(2,1)} async-done(((bf16[384,512]{1,0:T(8,128)(2,1)}), bf16[384,2048]{1,0:T(8,128)(2,1)}) %all-gather.8.cloned.1.call-update) | async-done | bytes 1572880 | tf_op jit(solution)/shard_map/all_gather | solution.py:140
  357.6 4.2 %fusion.36 = bf16[384,512]{1,0:T(8,128)(2,1)} fusion(f32[384,512]{1,0:T(8,128)} %convolution_multiply_fusion, f32[384,512]{1,0:T(8,128)} %fusion.29, bf16[384,2048]{1,0:T(8,128)(2,1)} %all-gather.8.cloned.1.call-done, bf16[2048,512]{1,0:T(8,128)(2,1)} %param.26), kind=kOutput, calls=%fused_computation.82 | convolution fusion | flops 805896192 | bytes 5636096 | tf_op jit(solution)/shard_map/dot_general | solution.py:142
  (32 shorter events, 0.2 us)
Async XLA Ops:
  7.2 26.6 %copy-start = (bf16[2048,512]{1,0:T(8,128)(2,1)S(1)}, bf16[2048,512]{1,0:T(8,128)(2,1)}, u32[]{:S(2)}) copy-start(bf16[2048,512]{1,0:T(8,128)(2,1)} %param.22) | copy-start | bytes 6291460
  7.2 24.8 %all-gather.6.cloned.1.call-start = ((), (), s32[]{:S(2)}) async-start(), calls=%async_computation | async-start | bytes 1966080 | tf_op jit(solution)/shard_map/all_gather | solution.py:61
  7.9 89.2 %all-gather.10.cloned.1.call-start = ((), (), s32[]{:S(2)}) async-start(), calls=%async_computation.2 | async-start | bytes 3538944 | tf_op jit(solution)/shard_map/all_gather | solution.py:97
  33.7 3.3 copy-start.8
  37.0 4.1 %copy-start.2 = (bf16[384,2048]{1,0:T(8,128)(2,1)S(1)}, bf16[384,2048]{1,0:T(8,128)(2,1)}, u32[]{:S(2)}) copy-start(bf16[384,2048]{1,0:T(8,128)(2,1)} %all-gather.6.cloned.1.call-done) | copy-start | bytes 4718596
  37.0 121.1 %all-gather.12.cloned.1.call-start = ((), (), s32[]{:S(2)}) async-start(), calls=%async_computation.3 | async-start | bytes 3538944 | tf_op jit(solution)/shard_map/all_gather | solution.py:96
  41.0 294.3 %all-gather.14.cloned.1.call-start = ((), (), s32[]{:S(2)}) async-start(), calls=%async_computation.4 | async-start | bytes 1966080 | tf_op jit(solution)/shard_map/all_gather | solution.py:141
  101.1 61.0 %copy-start.5 = (f32[8]{0:T(128)S(1)}, f32[8]{0:T(128)}, u32[]{:S(2)}) copy-start(f32[8]{0:T(128)} %param.23) | copy-start | bytes 100
  162.1 26.9 %copy-start.4 = (bf16[31,512]{1,0:T(8,128)(2,1)S(1)}, bf16[31,512]{1,0:T(8,128)(2,1)}, u32[]{:S(2)}) copy-start(bf16[31,512]{1,0:T(8,128)(2,1)} %param.24) | copy-start | bytes 95236
  188.7 168.9 %all-gather.8.cloned.1.call-start = ((), (), s32[]{:S(2)}) async-start(), calls=%async_computation.1 | async-start | bytes 1966080 | tf_op jit(solution)/shard_map/all_gather | solution.py:140
  189.1 3.4 copy-start.3
  189.1 3.4 copy-start.6
  193.5 29.7 %collective-permute-start = (bf16[30,512]{1,0:T(8,128)(2,1)S(1)}, bf16[30,512]{1,0:T(8,128)(2,1)S(1)}, u32[]{:S(2)}, u32[]{:S(2)}) collective-permute-start(bf16[30,512]{1,0:T(8,128)(2,1)S(1)} %slice.270), channel_id=1, source_target_pairs={{0,4},{4,8},{8,12},{12,16},{16,20},{20,24},{24,28},{1,5},{5,9},{9,... | collective-permute-start | bytes 92168 | tf_op jit(solution)/shard_map/ppermute | solution.py:14
  233.8 2.9 copy-start.7
  335.3 26.5 %copy-start.1 = (bf16[2048,512]{1,0:T(8,128)(2,1)S(1)}, bf16[2048,512]{1,0:T(8,128)(2,1)}, u32[]{:S(2)}) copy-start(bf16[2048,512]{1,0:T(8,128)(2,1)} %param.22) | copy-start | bytes 6291460
Sparse Core Ops, SparseCore 0:
  9.5 22.3 all-gather.5
  37.1 60.0 all-gather.9
  99.3 58.6 all-gather.11
  188.9 146.4 all-gather.13
  336.7 20.8 all-gather.7
where the time goes:
time: 369 us; the launch traced here: 368 us
  waiting for transfers between devices  250 us (68%)
  matrix products  34.1 us (9%)
  starting transfers between devices  28.5 us (8%)
  other arithmetic  23.9 us (6%)
  between operations  14 us (4%)
  local copies, waits for them, and re-layouts  11.9 us (3%)
  blocking collectives  5.67 us (2%)
    all_gather x1, waiting for transfers between devices, body(): attn_piece = lax.all_gather(attended, 'tp', axis=1, tiled=True)  96 us
    all_gather x1, waiting for transfers between devices, body(): lax.all_gather(keys, 'sp', axis=0, tiled=True)  57 us
    all_gather x1, waiting for transfers between devices, body(): lax.all_gather(values, 'sp', axis=0, tiled=True)  53.2 us
    ppermute x1, starting transfers between devices, passed_along(): return lax.ppermute(array, axis, pairs)  28.1 us
    all_gather x1, waiting for transfers between devices, body(): whole_rows = lax.all_gather(tokens, 'tp', axis=1, tiled=True)  24 us
    all_gather x1, waiting for transfers between devices, body(): conv_piece = lax.all_gather(conv_act, 'tp', axis=1, tiled=True)  18.2 us
    another operation x2, other arithmetic  15.2 us
  transfers between devices with their start and end apart: 6, of which 6 were waited for; matrix products, arithmetic and copies ran while one was open for 8% of the time, Pallas kernels for 0%

commit v1 on v0

--- a/solution.py
+++ b/solution.py
@@ -137,8 +137,11 @@
     conv_act = jax.nn.silu(
         (conv_float - channel_mean) * lax.rsqrt(channel_var + 1e-05) * local_gain
     ).astype(jnp.bfloat16)
-    conv_piece = lax.all_gather(conv_act, "tp", axis=1, tiled=True)
-    attn_piece = lax.all_gather(attended, "tp", axis=1, tiled=True)
+    conv_piece, attn_piece = jnp.split(
+        lax.all_gather(jnp.concatenate([conv_act, attended], axis=0), "tp", axis=1, tiled=True),
+        [conv_act.shape[0]],
+        axis=0,
+    )
     conv_branch = jnp.dot(conv_piece, w_conv_out, preferred_element_type=jnp.float32)
     attn_branch = jnp.dot(attn_piece, w_attn_out, preferred_element_type=jnp.float32)
     mixed = (gate_conv * conv_branch + gate_attn * attn_branch).astype(jnp.bfloat16)

time: 369 us -> 359 us (0.973)
  starting transfers between devices: 28.5 us -> 3.54 us
  waiting for transfers between devices: 250 us -> 268 us
  matrix products: 34.1 us -> 28.8 us
    all_gather x2 -> x1, waiting for transfers between devices: 114 us -> 149 us  [body(): lax.all_gather(jnp.concatenate([conv_act, attended], axis=0), 'tp', axis=...]
    ppermute x1, starting transfers between devices: 28.1 us -> 3.38 us  [passed_along(): return lax.ppermute(array, axis, pairs)]
    all_gather x1, waiting for transfers between devices: 57 us -> 36.4 us  [body(): lax.all_gather(keys, 'sp', axis=0, tiled=True)]
    all_gather x1, waiting for transfers between devices: 53.2 us -> 57.6 us  [body(): lax.all_gather(values, 'sp', axis=0, tiled=True)]
  transfers between devices with their start and end apart: 6 -> 5, of which waited for: 6 -> 5; matrix products, arithmetic and copies ran while one was open for 8% -> 7% of each run, Pallas kernels for 0% -> 0%
where the time goes in v1:
time: 359 us; the launch traced here: 358 us
  waiting for transfers between devices  268 us (75%)
  matrix products  28.8 us (8%)
  other arithmetic  23.4 us (7%)
  between operations  14 us (4%)
  local copies, waits for them, and re-layouts  13.2 us (4%)
  blocking collectives  6.32 us (2%)
    all_gather x1, waiting for transfers between devices, body(): lax.all_gather(jnp.concatenate([conv_act, attended], axis=0), 'tp', axis=...  149 us
    all_gather x1, waiting for transfers between devices, body(): lax.all_gather(values, 'sp', axis=0, tiled=True)  57.6 us
    all_gather x1, waiting for transfers between devices, body(): lax.all_gather(keys, 'sp', axis=0, tiled=True)  36.4 us
    all_gather x1, waiting for transfers between devices, body(): whole_rows = lax.all_gather(tokens, 'tp', axis=1, tiled=True)  24 us
    another operation x2, other arithmetic  15.2 us
  transfers between devices with their start and end apart: 5, of which 5 were waited for; matrix products, arithmetic and copies ran while one was open for 7% of the time, Pallas kernels for 0%

profile of v1, /device:TPU:0, one launch (start us, length us, event | category | flops | bytes accessed | tf_op | source)
XLA Modules:
  0.0 358.1 jit_solution(14598779131267737650)
XLA Ops:
  7.2 0.0 all-gather.5.cloned.1.call-start
  7.2 0.7 all-gather.5.cloned.1.call-update
  7.9 0.0 all-gather.9.cloned.1.call-start
  8.0 24.0 %all-gather.5.cloned.1.call-done = bf16[384,2048]{1,0:T(8,128)(2,1)} async-done(((bf16[384,512]{1,0:T(8,128)(2,1)}), bf16[384,2048]{1,0:T(8,128)(2,1)}) %all-gather.5.cloned.1.call-update) | async-done | bytes 1572880 | tf_op jit(solution)/shard_map/all_gather | solution.py:61
  31.9 1.8 fusion.22
  33.8 3.2 convolution_convert_fusion.1
  37.0 0.0 all-gather.9.cloned.1.call-update
  37.0 0.0 all-gather.7.cloned.1.call-start
  37.1 3.9 %convolution_convert_fusion.2 = bf16[384,512]{1,0:T(8,128)(2,1)} fusion(bf16[2048,512]{1,0:T(8,128)(2,1)} %param.22, bf16[384,2048]{1,0:T(8,128)(2,1)} %all-gather.5.cloned.1.call-done, f32[2048]{0:T(1024)S(1)} %copy-done.11, f32[384]{0:T(512)S(1)} %add_rsqrt_fusion), kind=kOutput, calls=%fused_computation.89 | convolution fusion | flops 808648704 | bytes 4072960 | tf_op jit(solution)/shard_map/dot_general | solution.py:74
  41.0 0.0 all-gather.7.cloned.1.call-update
  41.0 0.0 all-gather.11.cloned.1.call-start
  41.1 0.8 dynamic_slice.15
  41.9 2.9 fusion.41
  44.9 1.0 fusion.47
  45.9 3.4 collective-permute-start
  49.3 1.0 convolution_convert_fusion
  50.3 0.2 copy.26
  50.5 0.3 collective-permute-done
  50.9 3.7 %convert_reduce_fusion = (f32[384]{0:T(512)S(1)}, f32[384]{0:T(512)S(1)}, bf16[384,512]{1,0:T(8,128)(2,1)S(1)}) fusion(bf16[384,512]{1,0:T(8,128)(2,1)S(1)} %fusion.47, f32[512]{0:T(512)S(1)} %bitcast.130, bf16[30,512]{1,0:T(8,128)(2,1)S(1)} %collective-permute-done, f32[512]{0:T(512)S(1)} %bitcast.129, f32[512]{0:T(512)S(1)} %bitcast.128, ...), kind=kLoop, calls=%fused_computation.92 | loop fusion | flops 36764928 | bytes 883712 | tf_op jit(solution)/shard_map/reduce_sum | solution.py:129
  54.6 6.3 %all-reduce.2 = (f32[384,1]{0,1:T(1,128)S(1)}, f32[384,1]{0,1:T(1,128)S(1)}) all-reduce(f32[384,1]{0,1:T(1,128)S(1)} %broadcast_in_dim.41, f32[384,1]{0,1:T(1,128)S(1)} %broadcast_in_dim.42), channel_id=1, replica_groups=mesh['sp'=8,'tp'=4] {'tp'}, use_global_device_ids=true, to_apply=%region_2.3 | all-reduce | flops 768 | bytes 6144 | tf_op jit(solution)/shard_map/psum | solution.py:127
  61.0 0.3 fusion.58
  61.3 36.4 %all-gather.9.cloned.1.call-done = bf16[3072,512]{1,0:T(8,128)(2,1)} async-done(((bf16[384,512]{1,0:T(8,128)(2,1)}), bf16[3072,512]{1,0:T(8,128)(2,1)}) %all-gather.9.cloned.1.call-update) | async-done | bytes 3145744 | tf_op jit(solution)/shard_map/all_gather | solution.py:96
  97.7 3.9 %concatenate.14 = bf16[3584,512]{1,0:T(8,128)(2,1)} pad(bf16[3072,512]{1,0:T(8,128)(2,1)} %all-gather.9.cloned.1.call-done, bf16[]{:T(256)} %constant.89.clone.1), padding=512_0x0_0 | pad | bytes 6815746 | tf_op jit(solution)/shard_map/concatenate | solution.py:100
  101.6 57.6 %all-gather.7.cloned.1.call-done = bf16[3072,512]{1,0:T(8,128)(2,1)} async-done(((bf16[384,512]{1,0:T(8,128)(2,1)}), bf16[3072,512]{1,0:T(8,128)(2,1)}) %all-gather.7.cloned.1.call-update) | async-done | bytes 3145744 | tf_op jit(solution)/shard_map/all_gather | solution.py:97
  159.2 3.9 %concatenate.13 = bf16[3584,512]{1,0:T(8,128)(2,1)} pad(bf16[3072,512]{1,0:T(8,128)(2,1)} %all-gather.7.cloned.1.call-done, bf16[]{:T(256)} %constant.89.clone.1), padding=512_0x0_0 | pad | bytes 6815746 | tf_op jit(solution)/shard_map/concatenate | solution.py:101
  163.1 0.1 broadcast_in_dim.43
  163.2 26.0 %while.14 = (s32[]{:T(128)}, f32[384,8,64]{0,2,1:T(8,128)S(1)}, f32[8,384]{1,0:T(8,128)S(1)}, s32[]{:T(128)}, s32[]{:T(128)}, /*index=5*/bf16[3584,512]{1,0:T(8,...) while((s32[]{:T(128)}, f32[384,8,64]{0,2,1:T(8,128)S(1)}, ...), condition=%wide.region_8.9_spmd, body=%wide.region_5.8_spmd.sunk | while | flops 628213632 | bytes 71053592 | solution.py:120
  163.5 0.2 compare_and_fusion.2
  163.7 1.3 constant_dynamic-slice_fusion.3
  165.0 0.2 copy.44
  165.2 0.2 copy.45
  165.4 4.7 %fusion.124 = (f32[8,384,512]{1,2,0:T(8,128)S(1)}, f32[8,512,384]{2,1,0:T(8,128)S(1)}) fusion(f32[8]{0:T(128)S(1)} %get-tuple-element.322, pred[384,512]{0,1:T(8,128)(4,1)S(1)} %compare_and_fusion.2, bf16[512,8,64]{0,2,1:T(8,128)(2,1)S(1)} %bitcast.116, bf16[384,8,64]{0,2,1:T(8,128)(2,1)S(1)} %get-tuple-element.321), kind=kOutput, calls=%fused_computation.1.clone.1 | convolution fusion | flops 215482368 | bytes 13697056 | tf_op jit(solution)/shard_map/while/body/thd,shd->hts/dot_general | solution.py:27
  170.1 15.1 %fusion.125 = f32[8,384,4,128]{1,0,3,2:T(8,128)S(1)} fusion(f32[8,384,4,128]{1,3,2,0:T(8,128)S(1)} %bitcast.114), kind=kOutput, calls=%fused_computation.13.clone.1 | output fusion | flops 199753728 | bytes 12582912 | tf_op jit(solution)/shard_map/reduce-window.6
  185.2 0.1 fusion.126
  185.3 0.4 broadcast_add_fusion.2
  185.8 1.2 copy.46
  187.0 2.0 fusion.127
  189.3 0.2 copy.29
  189.5 0.9 pad_maximum_fusion
  190.5 0.0 all-gather.11.cloned.1.call-update
  190.5 0.5 copy-done.3
  191.0 2.9 fusion.43
  193.9 2.0 fusion.39
  195.9 0.6 negate_log_fusion
  196.6 149.4 %all-gather.11.cloned.1.call-done = bf16[768,2048]{1,0:T(8,128)(2,1)} async-done(((bf16[768,512]{1,0:T(8,128)(2,1)}), bf16[768,2048]{1,0:T(8,128)(2,1)}) %all-gather.11.cloned.1.call-update) | async-done | bytes 3145744 | tf_op jit(solution)/shard_map/all_gather | solution.py:141
  345.9 3.4 fusion.32
  349.3 0.5 copy-done.10
  349.8 1.7 fusion.48
  (37 shorter events, 0.3 us)
Async XLA Ops:
  7.2 26.6 %copy-start = (bf16[2048,512]{1,0:T(8,128)(2,1)S(1)}, bf16[2048,512]{1,0:T(8,128)(2,1)}, u32[]{:S(2)}) copy-start(bf16[2048,512]{1,0:T(8,128)(2,1)} %param.21) | copy-start | bytes 6291460
  7.2 24.8 %all-gather.5.cloned.1.call-start = ((), (), s32[]{:S(2)}) async-start(), calls=%async_computation | async-start | bytes 1966080 | tf_op jit(solution)/shard_map/all_gather | solution.py:61
  7.9 89.8 %all-gather.9.cloned.1.call-start = ((), (), s32[]{:S(2)}) async-start(), calls=%async_computation.2 | async-start | bytes 3538944 | tf_op jit(solution)/shard_map/all_gather | solution.py:96
  33.7 3.3 copy-start.11
  37.0 4.9 %copy-start.4 = (bf16[31,512]{1,0:T(8,128)(2,1)S(1)}, bf16[31,512]{1,0:T(8,128)(2,1)}, u32[]{:S(2)}) copy-start(bf16[31,512]{1,0:T(8,128)(2,1)} %param.24) | copy-start | bytes 95236
  37.0 4.9 %copy-start.2 = (bf16[384,2048]{1,0:T(8,128)(2,1)S(1)}, bf16[384,2048]{1,0:T(8,128)(2,1)}, u32[]{:S(2)}) copy-start(bf16[384,2048]{1,0:T(8,128)(2,1)} %all-gather.5.cloned.1.call-done) | copy-start | bytes 4718596
  37.0 122.2 %all-gather.7.cloned.1.call-start = ((), (), s32[]{:S(2)}) async-start(), calls=%async_computation.1 | async-start | bytes 3538944 | tf_op jit(solution)/shard_map/all_gather | solution.py:97
  41.0 304.9 %all-gather.11.cloned.1.call-start = ((), (), s32[]{:S(2)}) async-start(), calls=%async_computation.3 | async-start | bytes 3932160 | tf_op jit(solution)/shard_map/all_gather | solution.py:141
  41.9 2.9 copy-start.7
  44.8 4.5 %copy-start.8 = (bf16[2048,512]{1,0:T(8,128)(2,1)S(1)}, bf16[2048,512]{1,0:T(8,128)(2,1)}, u32[]{:S(2)}) copy-start(bf16[2048,512]{1,0:T(8,128)(2,1)} %param.20) | copy-start | bytes 6291460
  45.9 5.0 %collective-permute-start = (bf16[30,512]{1,0:T(8,128)(2,1)S(1)}, bf16[30,512]{1,0:T(8,128)(2,1)S(1)}, u32[]{:S(2)}, u32[]{:S(2)}) collective-permute-start(bf16[30,512]{1,0:T(8,128)(2,1)S(1)} %slice.270), channel_id=1, source_target_pairs={{0,4},{4,8},{8,12},{12,16},{16,20},{20,24},{24,28},{1,5},{5,9},{9,... | collective-permute-start | bytes 92168 | tf_op jit(solution)/shard_map/ppermute | solution.py:14
  101.6 61.6 %copy-start.5 = (f32[8]{0:T(128)S(1)}, f32[8]{0:T(128)}, u32[]{:S(2)}) copy-start(f32[8]{0:T(128)} %param.23) | copy-start | bytes 100
  189.3 1.7 copy-start.3
  191.0 2.9 copy-start.9
  345.9 3.4 copy-start.6
  345.9 3.9 %copy-start.10 = (bf16[2048,512]{1,0:T(8,128)(2,1)S(1)}, bf16[2048,512]{1,0:T(8,128)(2,1)}, u32[]{:S(2)}) copy-start(bf16[2048,512]{1,0:T(8,128)(2,1)} %param.27) | copy-start | bytes 6291460
  345.9 5.6 %copy-start.1 = (bf16[2048,512]{1,0:T(8,128)(2,1)S(1)}, bf16[2048,512]{1,0:T(8,128)(2,1)}, u32[]{:S(2)}) copy-start(bf16[2048,512]{1,0:T(8,128)(2,1)} %param.21) | copy-start | bytes 6291460
Sparse Core Ops, SparseCore 0:
  9.5 22.3 all-gather.4
  37.1 60.5 all-gather.8
  100.5 58.6 all-gather.6
  190.6 155.2 all-gather.10
